TPU v7x, 512 devices: a whole 4x8x8 slice. The times are simulated.
512 devices in a mesh: sp: 32 (over z, x), tp: 16 (over y, core).
Axes of the slice: x: 4, y: 8, z: 8, core: 2. Of those that a mesh axis runs over, the one named last changes fastest.
Arguments:
- resid: bfloat16 [16384, 2048], P(('sp', 'tp')), may hold values from -6 to 6
- recurrent_input: bfloat16 [16384, 2048], P('sp', 'tp'), may hold values from -12.2 to 12.2
- recurrent_out_gate: bfloat16 [16384, 2048], P('sp', 'tp'), may hold values from -6 to 6
- filter_weight: float32 [4, 2048], P(None, 'tp'), may hold values from -3 to 3
- recurrence_gate_matrix: bfloat16 [32, 64, 64], P('tp'), may hold values from -0.75 to 0.75
- input_gate_matrix: bfloat16 [32, 64, 64], P('tp'), may hold values from -0.75 to 0.75
- channel_decay_raw: float32 [2048], P('tp'), may hold values from 4.8 to 13.5
- token_decay_boost: float32 [16384, 2048], P('sp', 'tp'), may hold values from -0.7 to 0
- output_projection_weight: bfloat16 [2048, 2048], P('tp'), may hold values from -0.375 to 0.375
- expert_norm_gain: float32 [2048], replicated, may hold values from 0.1 to 1.9
- routes: int32 [16384, 2], P('sp'), may hold values from 0 to 31, all different within a row; in each aligned block of 32 rows (0 to 31, 32 to 63, ...) at most 3 rows name the same one
- expert_pair_weight: float32 [16384, 2], P(('sp', 'tp')), may hold values from 0.2 to 0.8
- gate_weight: bfloat16 [32, 2048, 2048], P('sp', None, 'tp'), may hold values from -0.125 to 0.125
- up_weight: bfloat16 [32, 2048, 2048], P('sp', None, 'tp'), may hold values from -0.125 to 0.125
- down_weight: bfloat16 [32, 2048, 2048], P('sp', None, 'tp'), may hold values from -0.25 to 0.25
Outputs:
- layer_out: bfloat16 [16384, 2048], P(('sp', 'tp'))
Inputs may be any that keep to these rules, and one draw needn't show every extreme that they name: `routes`: in each aligned block of 32 rows no expert is named by more than 3 rows, and the two experts of a row differ.
All inputs are finite; a program needn't handle non-finite values.
Results may differ from a plain program's by a relative error of at most 0.013.
Values may be sent and summed in bfloat16 or wider, within the bound.
No kernel may reach another device: no remote copies, remote signals or barrier semaphores. Data moves between devices by JAX's collectives and lax.ppermute only.
A program may use at most 64 MiB of HBM per device.

v0:
```python
import jax
import jax.numpy as jnp
from jax import lax
from jax.sharding import PartitionSpec as P

RECURRENT_SCALE = 8.0
EPSILON = 1e-06


def shifted(block, axis, distance):
    devices = range(lax.axis_size(axis))
    route = [(i - distance, i) for i in devices if i - distance in devices]
    return lax.ppermute(block, axis, route)


def from_everyone(x, axis):
    size = lax.axis_size(axis)
    return lax.all_to_all(jnp.broadcast_to(x[None], (size, *x.shape)), axis, 0, 0, tiled=True)


def collected_together(x, axis):
    leaves = jax.tree.leaves(x)
    order = sorted(range(len(leaves)), key=lambda k: -leaves[k].size)
    width = (1, *leaves[order[0]].shape)[-1]
    lines = [
        jnp.pad(leaves[k].reshape(-1), (0, -leaves[k].size % width)).reshape(-1, width)
        for k in order
    ]
    both, at, found = (from_everyone(jnp.concatenate(lines), axis), 0, {})
    for k, line in zip(order, lines):
        slab = both[:, at : at + len(line)].reshape(len(both), -1)
        found[k] = slab[:, : leaves[k].size].reshape(-1, *leaves[k].shape)
        at += len(line)
    numbers = iter(range(len(leaves)))
    return jax.tree.map(lambda _: found[next(numbers)], x)


def joined_by_halves(pieces, combine):
    while len(jax.tree.leaves(pieces)[0]) > 1:
        pieces = jax.vmap(combine)(
            *(jax.tree.map(lambda part: part[side::2], pieces) for side in (0, 1))
        )
    return jax.tree.map(lambda part: part[0], pieces)


def carried_in(x, axis, combine, identity):
    size, position = (lax.axis_size(axis), lax.axis_index(axis))
    passed = jnp.arange(size) < position

    def kept(part, zero, own):
        part = jnp.where(
            passed.reshape(-1, *(1 for _ in own.shape)), part, jnp.asarray(zero, own.dtype)
        )
        return part

    pieces = collected_together(x, axis)
    return joined_by_halves(jax.tree.map(kept, pieces, identity, x), combine)


def split_up(x, dim, size):
    before, after = (x.shape[:dim], x.shape[dim + 1 :])
    return jnp.moveaxis(x.reshape(*before, size, -1, *after), dim, 0)


def sum_at_owner(x, axis, dim):
    pieces = split_up(x, dim, lax.axis_size(axis))
    arrived = lax.all_to_all(pieces, axis, split_axis=0, concat_axis=0, tiled=True)
    return arrived.astype(jnp.float32).sum(axis=0)


def in_order(pieces, dim):
    pieces = jnp.moveaxis(pieces, 0, dim)
    dims = pieces.shape
    return pieces.reshape(*dims[:dim], dims[dim] * dims[dim + 1], *dims[dim + 2 :])


def piecewise(x, axis, dim, work, out_dim):
    extent = x.shape[dim]
    pieces = jnp.split(x, 2, axis=dim) if extent % 2 == 0 else [x]
    first = jnp.arange(lax.axis_size(axis)) * extent
    blocks = [lax.all_gather(slab, axis) for slab in pieces]
    made = [jax.vmap(work)(b, first + k * (extent // len(pieces))) for k, b in enumerate(blocks)]
    return in_order(jnp.concatenate(made, axis=out_dim + 1), out_dim)


def chain_step(earlier, later):
    return (earlier[0] * later[0], later[0] * earlier[1] + later[1])


def slot_numbers(picks, experts):
    flat = picks.reshape(-1)
    onehot = (flat[:, None] == jnp.arange(experts, dtype=jnp.int32)[None, :]).astype(jnp.int32)
    before = jnp.cumsum(onehot, axis=0) - onehot
    return (flat, jnp.sum(before * onehot, axis=1))


def fill_slots(source_rows, slot_of, row_of, slot_count):
    match = slot_of[None, :] == jnp.arange(slot_count, dtype=jnp.int32)[:, None]
    picked = jnp.sum(jnp.where(match, row_of[None, :], 0), axis=1)
    present = jnp.any(match, axis=1)
    return jnp.where(present[:, None], source_rows[picked], jnp.zeros((), source_rows.dtype))


def expert_hidden(rows, gate_weight, up_weight):
    gate = jnp.dot(rows, gate_weight[0], preferred_element_type=jnp.float32)
    upward = jnp.dot(rows, up_weight[0], preferred_element_type=jnp.float32)
    return (jax.nn.silu(gate) * upward).astype(jnp.bfloat16)


def expert_down(active, down_weight):
    columns = down_weight[0]
    return jnp.dot(
        lax.all_gather(active, "tp", axis=1, tiled=True),
        columns,
        preferred_element_type=jnp.float32,
    ).astype(jnp.bfloat16)


def body(
    resid,
    recurrent_input,
    recurrent_out_gate,
    filter_weight,
    recurrence_gate_matrix,
    input_gate_matrix,
    channel_decay_raw,
    token_decay_boost,
    output_projection_weight,
    expert_norm_gain,
    routes,
    expert_pair_weight,
    gate_weight,
    up_weight,
    down_weight,
):
    tokens_here, channels = recurrent_input.shape
    taps = filter_weight.shape[0]
    rim = shifted(recurrent_input[tokens_here - taps + 1 :], "sp", 1)
    extended = jnp.concatenate([rim, recurrent_input], axis=0).astype(jnp.float32)
    mixed_in = extended[0:tokens_here] * filter_weight[0]
    for offset in range(1, taps):
        mixed_in = mixed_in + extended[offset : offset + tokens_here] * filter_weight[offset]
    smoothed = mixed_in.astype(jnp.bfloat16)
    grouped = smoothed.reshape(
        tokens_here, recurrence_gate_matrix.shape[0], recurrence_gate_matrix.shape[1]
    )
    recurrence_gate = jax.nn.sigmoid(
        jnp.einsum(
            "tni,nij->tnj", grouped, recurrence_gate_matrix, preferred_element_type=jnp.float32
        ).reshape(tokens_here, channels)
    )
    input_gate = jax.nn.sigmoid(
        jnp.einsum(
            "tni,nij->tnj", grouped, input_gate_matrix, preferred_element_type=jnp.float32
        ).reshape(tokens_here, channels)
    )
    decay_logarithm = (
        -RECURRENT_SCALE * recurrence_gate * jax.nn.softplus(-channel_decay_raw) + token_decay_boost
    )
    decay = jnp.exp(decay_logarithm)
    drive = jnp.sqrt(-jnp.expm1(2.0 * decay_logarithm)) * (
        input_gate * smoothed.astype(jnp.float32)
    )
    running, local_state = lax.associative_scan(chain_step, (decay, drive), axis=0)
    identity = (jnp.ones((channels,), jnp.float32), jnp.zeros((channels,), jnp.float32))
    carried = carried_in((running[-1], local_state[-1]), "sp", chain_step, identity)
    state = local_state + running * carried[1][None, :]
    branch = (jax.nn.gelu(recurrent_out_gate.astype(jnp.float32)) * state).astype(jnp.bfloat16)
    tp_size = lax.axis_size("tp")
    rows_dev = tokens_here // tp_size
    projected = sum_at_owner(
        jnp.dot(branch, output_projection_weight, preferred_element_type=jnp.float32).astype(
            jnp.bfloat16
        ),
        "tp",
        0,
    )
    stream = (resid.astype(jnp.float32) + projected).astype(jnp.bfloat16)
    stream_wide = stream.astype(jnp.float32)
    normed = (
        stream_wide
        * lax.rsqrt(jnp.mean(stream_wide * stream_wide, axis=1, keepdims=True) + EPSILON)
        * expert_norm_gain
    ).astype(jnp.bfloat16)
    model_width = normed.shape[1]
    experts = lax.axis_size("sp")
    capacity = max(2, 3 * rows_dev // experts)
    own_routes = lax.dynamic_slice_in_dim(routes, lax.axis_index("tp") * rows_dev, rows_dev, 0)
    own_flat, own_rank = slot_numbers(own_routes, experts)
    own_slots = own_flat * capacity + own_rank
    row_of = jnp.arange(2 * rows_dev, dtype=jnp.int32) // 2
    outgoing = fill_slots(normed, own_slots, row_of, experts * capacity).reshape(
        experts, capacity, model_width
    )
    arrived = lax.all_to_all(outgoing, "sp", split_axis=0, concat_axis=0, tiled=True)

    def hidden_piece(piece, start):
        flat_rows = piece.reshape(piece.shape[0] * piece.shape[1], model_width)
        return expert_hidden(flat_rows, gate_weight, up_weight).reshape(
            piece.shape[0], piece.shape[1], -1
        )

    active = piecewise(
        arrived.reshape(1, experts * capacity, model_width), "tp", 0, hidden_piece, 0
    )
    result = expert_down(active.reshape(-1, active.shape[2]), down_weight)
    joined = lax.all_to_all(
        result.reshape(tp_size, experts * capacity, -1),
        "tp",
        split_axis=0,
        concat_axis=2,
        tiled=True,
    )
    returned = lax.all_to_all(
        joined.reshape(experts, capacity, model_width),
        "sp",
        split_axis=0,
        concat_axis=0,
        tiled=True,
    )
    picked = (
        returned.reshape(experts * capacity, model_width)[own_slots]
        .astype(jnp.float32)
        .reshape(rows_dev, 2, model_width)
    )
    blended = jnp.sum(picked * expert_pair_weight[:, :, None], axis=1)
    return (stream_wide + blended).astype(jnp.bfloat16)


def solution(mesh):
    placed = (
        P(("sp", "tp"), None),
        P("sp", "tp"),
        P("sp", "tp"),
        P(None, "tp"),
        P("tp", None, None),
        P("tp", None, None),
        P("tp"),
        P("sp", "tp"),
        P("tp", None),
        P(),
        P("sp", None),
        P(("sp", "tp"), None),
        P("sp", None, "tp"),
        P("sp", None, "tp"),
        P("sp", None, "tp"),
    )
    return jax.shard_map(
        body, mesh=mesh, in_specs=placed, out_specs=P(("sp", "tp"), None), check_vma=False
    )
```

profile of v0, /device:TPU:1, one launch (start us, length us, event | category | flops | bytes accessed | tf_op | source)
XLA Modules:
  0.0 395.7 jit_solution(9061123407506774359)
XLA Ops:
  6.5 0.7 slice.359
  7.4 3.9 collective-permute-start
  11.4 0.8 slice_bitcast_fusion.3
  12.2 0.7 fusion.50
  12.9 1.0 copy.85
  13.9 1.1 copy.87
  15.0 1.0 copy.83
  16.5 1.0 fusion.12
  17.5 1.0 fusion.15
  19.0 4.5 %slice.371 = f32[256,128]{0,1:T(8,128)S(1)} slice(f32[512,128]{0,1:T(8,128)S(1)} %get-tuple-element.9), slice={[0:511:2], [0:128:1]} | slice | bytes 262144 | tf_op jit(solution)/shard_map/slice | solution.py:164
  23.5 4.5 %slice.372 = f32[256,128]{0,1:T(8,128)S(1)} slice(f32[512,128]{0,1:T(8,128)S(1)} %get-tuple-element.9), slice={[1:512:2], [0:128:1]} | slice | bytes 262144 | tf_op jit(solution)/shard_map/slice | solution.py:164
  27.9 4.5 %slice.370 = f32[256,128]{0,1:T(8,128)S(1)} slice(f32[512,128]{0,1:T(8,128)S(1)} %get-tuple-element.10), slice={[1:512:2], [0:128:1]} | slice | bytes 262144 | tf_op jit(solution)/shard_map/slice | solution.py:164
  32.4 5.0 %slice.374 = f32[256,128]{0,1:T(8,128)S(1)} slice(f32[512,128]{0,1:T(8,128)S(1)} %get-tuple-element.10), slice={[0:511:2], [0:128:1]} | slice | bytes 262144 | tf_op jit(solution)/shard_map/slice | solution.py:164
  37.5 2.2 slice.377
  39.7 2.2 slice.378
  41.9 2.2 slice.376
  44.1 2.2 slice.380
  46.3 1.1 slice.383
  47.5 1.2 slice.384
  48.6 1.2 slice.382
  49.8 1.1 slice.386
  52.2 0.8 slice.388
  57.0 0.8 add_multiply_fusion.15
  60.3 1.1 slice.381
  61.5 1.1 slice.430
  62.6 2.2 slice.375
  64.8 2.2 slice.432
  67.1 4.5 %slice.369 = f32[255,128]{0,1:T(8,128)S(1)} slice(f32[512,128]{0,1:T(8,128)S(1)} %get-tuple-element.10), slice={[2:512:2], [0:128:1]} | slice | bytes 261120 | tf_op jit(solution)/shard_map/slice | solution.py:164
  71.5 4.9 %slice.434 = f32[255,128]{0,1:T(8,128)S(1)} slice(f32[512,128]{0,1:T(8,128)S(1)} %get-tuple-element.9), slice={[2:512:2], [0:128:1]} | slice | bytes 261120 | tf_op jit(solution)/shard_map/slice | solution.py:164
  76.5 0.9 copy.113
  84.9 1.1 pad.140
  86.0 1.1 pad.141
  87.2 1.1 pad.123
  88.4 1.1 pad.122
  89.7 2.2 pad.142
  91.9 2.2 pad.143
  94.1 4.5 %pad.145 = f32[512,128]{0,1:T(8,128)S(1)} pad(f32[256,128]{0,1:T(8,128)S(1)} %add.346, f32[]{:T(128)} %constant.25.clone.1), padding=1_0_1x0_0_0 | pad | bytes 393220 | tf_op jit(solution)/shard_map/pad | solution.py:164
  98.7 2.2 pad.124
  100.9 2.2 pad.125
  103.3 4.4 %pad.144 = f32[512,128]{0,1:T(8,128)S(1)} pad(f32[256,128]{0,1:T(8,128)S(1)} %pad_maximum_fusion.1, f32[]{:T(128)} %constant.25.clone.1), padding=0_1_1x0_0_0 | pad | bytes 393220 | tf_op jit(solution)/shard_map/pad | solution.py:164
  107.9 4.6 %pad.127 = f32[512,128]{0,1:T(8,128)S(1)} pad(f32[256,128]{0,1:T(8,128)S(1)} %add.336, f32[]{:T(128)} %constant.25.clone.1), padding=1_0_1x0_0_0 | pad | bytes 393220 | tf_op jit(solution)/shard_map/pad | solution.py:164
  112.6 4.4 %pad.126 = f32[512,128]{0,1:T(8,128)S(1)} pad(f32[256,128]{0,1:T(8,128)S(1)} %pad_maximum_fusion, f32[]{:T(128)} %constant.25.clone.1), padding=0_1_1x0_0_0 | pad | bytes 393220 | tf_op jit(solution)/shard_map/pad | solution.py:164
  117.1 0.6 broadcast_in_dim.64
  117.8 12.6 %all-to-all-start = ((f32[32,2,128]{2,1,0:T(2,128)}), f32[32,2,128]{2,1,0:T(2,128)S(1)}, u32[]{:S(2)}, u32[]{:S(2)}) async-start(f32[32,2,128]{2,1,0:T(2,128)} %broadcast_in_dim.64), calls=%async_computation | async-start | bytes 65536 | tf_op jit(solution)/shard_map/all_to_all | solution.py:18
  130.4 8.7 %all-to-all-done = f32[32,2,128]{2,1,0:T(2,128)S(1)} async-done(((f32[32,2,128]{2,1,0:T(2,128)}), f32[32,2,128]{2,1,0:T(2,128)S(1)}, u32[]{:S(2)}, u32[]{:S(2)}) %all-to-all-start) | async-done | bytes 32800 | tf_op jit(solution)/shard_map/all_to_all | solution.py:18
  139.5 2.2 convolution_convert_fusion
  141.7 9.5 %all-to-all-start.1 = ((bf16[16,32,2048]{2,1,0:T(8,128)(2,1)}), bf16[16,32,2048]{2,1,0:T(8,128)(2,1)S(1)}, u32[]{:S(2)}, u32[]{:S(2)}) async-start(bf16[16,32,2048]{2,1,0:T(8,128)(2,1)} %bitcast.12), calls=%async_computation.1 | async-start | bytes 4194304 | tf_op jit(solution)/shard_map/all_to_all | solution.py:67
  151.2 0.8 broadcast_multiply_fusion
  152.9 47.3 %all-to-all-done.1 = bf16[16,32,2048]{2,1,0:T(8,128)(2,1)S(1)} async-done(((bf16[16,32,2048]{2,1,0:T(8,128)(2,1)}), bf16[16,32,2048]{2,1,0:T(8,128)(2,1)S(1)}, u32[]{:S(2)}, u32[]{:S(2)}) %all-to-all-start.1) | async-done | bytes 2097184 | tf_op jit(solution)/shard_map/all_to_all | solution.py:67
  200.9 0.8 gather_fusion
  202.3 19.6 %all_to_all.35 = bf16[32,3,2048]{2,1,0:T(4,128)(2,1)S(1)} all-to-all(bf16[32,3,2048]{2,1,0:T(4,128)(2,1)S(1)} %broadcast_select_fusion), channel_id=1, replica_groups=mesh['sp'=32,'tp'=16] {'sp'}, dimensions={0} | all-to-all | bytes 786432 | tf_op jit(solution)/shard_map/all_to_all | solution.py:195
  221.9 1.1 all_gather_reshape.3
  223.3 43.7 %all-gather.3.cloned.1.call-done = bf16[16,1,96,2048]{3,2,1,0:T(8,128)(2,1)} async-done(((bf16[1,1,96,2048]{3,2,1,0:T(8,128)(2,1)}), bf16[16,1,96,2048]{3,2,1,0:T(8,128)(2,1)}) %all-gather.3.cloned.1.call-update) | async-done | bytes 6291472 | tf_op jit(solution)/shard_map/all_gather | solution.py:81
  267.0 4.7 %fusion.2 = f32[16,96,128]{2,1,0:T(8,128)S(1)} fusion(bf16[16,1,96,2048]{3,2,1,0:T(8,128)(2,1)} %all-gather.3.cloned.1.call-done, bf16[1,2048,128]{2,1,0:T(8,128)(2,1)S(1)} %copy-done.5), kind=kOutput, calls=%fused_computation.4 | convolution fusion | flops 805306368 | bytes 7602176 | tf_op jit(solution)/shard_map/vmap()/dot_general | solution.py:105
  271.7 2.6 fusion.7
  274.4 58.5 %all-gather.5.cloned.1.call-done = bf16[1536,2048]{1,0:T(8,128)(2,1)} async-done(((bf16[1536,128]{1,0:T(8,128)(2,1)}), bf16[1536,2048]{1,0:T(8,128)(2,1)}) %all-gather.5.cloned.1.call-update) | async-done | bytes 6291472 | tf_op jit(solution)/shard_map/all_gather | solution.py:113
  332.9 4.6 %convolution_convert_fusion.1 = bf16[1536,128]{1,0:T(8,128)(2,1)S(1)} fusion(bf16[1536,2048]{1,0:T(8,128)(2,1)} %all-gather.5.cloned.1.call-done, bf16[1,2048,128]{2,1,0:T(8,128)(2,1)S(1)} %copy-done.7), kind=kOutput, calls=%fused_computation.8 | convolution fusion | flops 805502976 | bytes 7208960 | tf_op jit(solution)/shard_map/dot_general | solution.py:112
  337.5 19.4 %all_to_all.36 = bf16[16,96,128]{2,1,0:T(8,128)(2,1)S(1)} all-to-all(bf16[16,96,128]{2,1,0:T(8,128)(2,1)S(1)} %bitcast.97), channel_id=1, replica_groups=mesh['sp'=32,'tp'=16] {'tp'}, dimensions={0} | all-to-all | bytes 786432 | tf_op jit(solution)/shard_map/all_to_all | solution.py:207
  357.0 0.9 reshape.148
  357.9 9.9 %all-to-all-start.4 = ((bf16[32,3,2048]{2,1,0:T(4,128)(2,1)}), bf16[32,3,2048]{2,1,0:T(4,128)(2,1)S(1)}, u32[]{:S(2)}, u32[]{:S(2)}) async-start(bf16[32,3,2048]{2,1,0:T(4,128)(2,1)} %reshape.148), calls=%async_computation.4 | async-start | bytes 1048576 | tf_op jit(solution)/shard_map/all_to_all | solution.py:214
  368.2 17.4 %all-to-all-done.4 = bf16[32,3,2048]{2,1,0:T(4,128)(2,1)S(1)} async-done(((bf16[32,3,2048]{2,1,0:T(4,128)(2,1)}), bf16[32,3,2048]{2,1,0:T(4,128)(2,1)S(1)}, u32[]{:S(2)}, u32[]{:S(2)}) %all-to-all-start.4) | async-done | bytes 393248 | tf_op jit(solution)/shard_map/all_to_all | solution.py:214
  385.9 0.7 gather_fusion.1
  387.0 0.7 multiply_reduce_fusion
  387.7 0.7 fusion.22
  (191 shorter events, 20.8 us)
Async XLA Ops:
  6.5 133.0 %copy-start = (bf16[128,2048]{1,0:T(8,128)(2,1)S(1)}, bf16[128,2048]{1,0:T(8,128)(2,1)}, u32[]{:S(2)}) copy-start(bf16[128,2048]{1,0:T(8,128)(2,1)} %param.23) | copy-start | bytes 1572868
  7.4 8.6 %collective-permute-start = (bf16[3,128]{0,1:T(8,128)(2,1)S(1)}, bf16[3,128]{0,1:T(8,128)(2,1)S(1)}, u32[]{:S(2)}, u32[]{:S(2)}) collective-permute-start(bf16[3,128]{0,1:T(8,128)(2,1)S(1)} %copy.84), channel_id=1, source_target_pairs={{0,16},{16,32},{32,48},{48,64},{64,80},{80,96},{96,112},{112,128},... | collective-permute-start | bytes 2312 | tf_op jit(solution)/shard_map/ppermute | solution.py:13
  107.8 92.8 %copy-start.1 = (bf16[32,2048]{1,0:T(8,128)(2,1)S(1)}, bf16[32,2048]{1,0:T(8,128)(2,1)}, u32[]{:S(2)}) copy-start(bf16[32,2048]{1,0:T(8,128)(2,1)} %param.15) | copy-start | bytes 393220
  112.4 88.3 %copy-start.2 = (f32[2048]{0:T(1024)S(1)}, f32[2048]{0:T(1024)}, u32[]{:S(2)}) copy-start(f32[2048]{0:T(1024)} %param.24) | copy-start | bytes 24580
  117.8 21.3 %all-to-all-start = ((f32[32,2,128]{2,1,0:T(2,128)}), f32[32,2,128]{2,1,0:T(2,128)S(1)}, u32[]{:S(2)}, u32[]{:S(2)}) async-start(f32[32,2,128]{2,1,0:T(2,128)} %broadcast_in_dim.64), calls=%async_computation | async-start | bytes 65536 | tf_op jit(solution)/shard_map/all_to_all | solution.py:18
  141.7 58.5 %all-to-all-start.1 = ((bf16[16,32,2048]{2,1,0:T(8,128)(2,1)}), bf16[16,32,2048]{2,1,0:T(8,128)(2,1)S(1)}, u32[]{:S(2)}, u32[]{:S(2)}) async-start(bf16[16,32,2048]{2,1,0:T(8,128)(2,1)} %bitcast.12), calls=%async_computation.1 | async-start | bytes 4194304 | tf_op jit(solution)/shard_map/all_to_all | solution.py:67
  151.2 115.8 %copy-start.5 = (bf16[1,2048,128]{2,1,0:T(8,128)(2,1)S(1)}, bf16[1,2048,128]{2,1,0:T(8,128)(2,1)}, u32[]{:S(2)}) copy-start(bf16[1,2048,128]{2,1,0:T(8,128)(2,1)} %param.27) | copy-start | bytes 1572868
  151.2 115.8 %all-gather.3.cloned.1.call-start = ((), (), s32[]{:S(2)}) async-start(), calls=%async_computation.5 | async-start | bytes 6684672 | tf_op jit(solution)/shard_map/all_gather | solution.py:81
  223.0 48.8 %copy-start.6 = (bf16[1,2048,128]{2,1,0:T(8,128)(2,1)S(1)}, bf16[1,2048,128]{2,1,0:T(8,128)(2,1)}, u32[]{:S(2)}) copy-start(bf16[1,2048,128]{2,1,0:T(8,128)(2,1)} %param.28) | copy-start | bytes 1572868
  223.0 109.9 %all-gather.5.cloned.1.call-start = ((), (), s32[]{:S(2)}) async-start(), calls=%async_computation.6 | async-start | bytes 6684672 | tf_op jit(solution)/shard_map/all_gather | solution.py:113
  267.0 4.8 %copy-start.4 = (bf16[16,1,96,2048]{3,2,1,0:T(8,128)(2,1)S(1)}, bf16[16,1,96,2048]{3,2,1,0:T(8,128)(2,1)}, u32[]{:S(2)}) copy-start(bf16[16,1,96,2048]{3,2,1,0:T(8,128)(2,1)} %all-gather.3.cloned.1.call-done) | copy-start | bytes 18874372
  271.7 61.1 %copy-start.7 = (bf16[1,2048,128]{2,1,0:T(8,128)(2,1)S(1)}, bf16[1,2048,128]{2,1,0:T(8,128)(2,1)}, u32[]{:S(2)}) copy-start(bf16[1,2048,128]{2,1,0:T(8,128)(2,1)} %param.29) | copy-start | bytes 1572868
  274.3 93.7 %copy-start.3 = (f32[32,2]{0,1:T(2,128)S(1)}, f32[32,2]{0,1:T(2,128)}, u32[]{:S(2)}) copy-start(f32[32,2]{0,1:T(2,128)} %param.26) | copy-start | bytes 772
  357.9 27.6 %all-to-all-start.4 = ((bf16[32,3,2048]{2,1,0:T(4,128)(2,1)}), bf16[32,3,2048]{2,1,0:T(4,128)(2,1)S(1)}, u32[]{:S(2)}, u32[]{:S(2)}) async-start(bf16[32,3,2048]{2,1,0:T(4,128)(2,1)} %reshape.148), calls=%async_computation.4 | async-start | bytes 1048576 | tf_op jit(solution)/shard_map/all_to_all | solution.py:214
Sparse Core Ops, SparseCore 0:
  223.1 43.8 all-gather.2
  274.5 58.3 all-gather.4
where the time goes:
time: 403 us; the launch traced here: 396 us
  waiting for transfers between devices  176 us (44%)
  local copies, waits for them, and re-layouts  105 us (26%)
  blocking collectives  39 us (10%)
  starting transfers between devices  36.2 us (9%)
  matrix products  16.1 us (4%)
  between operations  15.1 us (4%)
  other arithmetic  8.3 us (2%)
    all_gather x1, waiting for transfers between devices, expert_down(): lax.all_gather(active, 'tp', axis=1, tiled=True)  58.5 us
    slice x50, local copies, waits for them, and re-layouts, body(): lax.associative_scan(chain_step, (decay, drive), axis=0)  56 us
    all_to_all x1, waiting for transfers between devices, sum_at_owner(): lax.all_to_all(pieces, axis, split_axis=0, concat_axis=0, tiled=True)  47.3 us
    all_gather x1, waiting for transfers between devices, piecewise(): blocks = [lax.all_gather(slab, axis) for slab in pieces]  43.7 us
    pad x32, local copies, waits for them, and re-layouts, body(): lax.associative_scan(chain_step, (decay, drive), axis=0)  36.4 us
    all_to_all x1, blocking collectives, body(): lax.all_to_all(outgoing, 'sp', split_axis=0, concat_axis=0, tiled=True)  19.6 us
    all_to_all x1, blocking collectives, body(): lax.all_to_all(result.reshape(tp_size, experts * capacity, -1), 'tp', spl...  19.4 us
    all_to_all x1, waiting for transfers between devices, body(): lax.all_to_all(joined.reshape(experts, capacity, model_width), 'sp', spli...  17.4 us
  transfers between devices with their start and end apart: 6, of which 5 were waited for; matrix products, arithmetic and copies ran while one was open for 2% of the time, Pallas kernels for 0%

commit v1 on v0

--- a/solution.py
+++ b/solution.py
@@ -110,7 +110,9 @@
 def expert_down(active, down_weight):
     columns = down_weight[0]
     return jnp.dot(
-        lax.all_gather(active, "tp", axis=1, tiled=True),
+        jnp.concatenate(
+            lax.all_to_all(jnp.stack([active] * lax.axis_size("tp")), "tp", 0, 0), axis=1
+        ),
         columns,
         preferred_element_type=jnp.float32,
     ).astype(jnp.bfloat16)

time: 403 us -> 485 us (1.20)
  blocking collectives: 39 us -> 182 us
  waiting for transfers between devices: 176 us -> 117 us
    all_to_all x0 -> x1, blocking collectives: none -> 145 us  [expert_down(): lax.all_to_all(jnp.stack([active] * lax.axis_size('tp')), 'tp', 0, 0)]
    all_gather x1 -> x0, waiting for transfers between devices: 58.5 us -> none  [expert_down(): lax.all_gather(active, 'tp', axis=1, tiled=True)]
  transfers between devices with their start and end apart: 6 -> 5, of which waited for: 5 -> 4; matrix products, arithmetic and copies ran while one was open for 2% -> 1% of each run, Pallas kernels for 0% -> 0%
where the time goes in v1:
time: 485 us; the launch traced here: 478 us
  blocking collectives  182 us (38%)
  waiting for transfers between devices  117 us (24%)
  local copies, waits for them, and re-layouts  106 us (22%)
  starting transfers between devices  35.9 us (7%)
  between operations  15.1 us (3%)
  matrix products  12.6 us (3%)
  other arithmetic  8.3 us (2%)
    all_to_all x1, blocking collectives, expert_down(): lax.all_to_all(jnp.stack([active] * lax.axis_size('tp')), 'tp', 0, 0)  145 us
    slice x50, local copies, waits for them, and re-layouts, body(): lax.associative_scan(chain_step, (decay, drive), axis=0)  56 us
    all_to_all x1, waiting for transfers between devices, sum_at_owner(): lax.all_to_all(pieces, axis, split_axis=0, concat_axis=0, tiled=True)  47.3 us
    all_gather x1, waiting for transfers between devices, piecewise(): blocks = [lax.all_gather(slab, axis) for slab in pieces]  44 us
    pad x32, local copies, waits for them, and re-layouts, body(): lax.associative_scan(chain_step, (decay, drive), axis=0)  36.4 us
    all_to_all x1, blocking collectives, body(): lax.all_to_all(outgoing, 'sp', split_axis=0, concat_axis=0, tiled=True)  19.9 us
    all_to_all x1, waiting for transfers between devices, body(): lax.all_to_all(joined.reshape(experts, capacity, model_width), 'sp', spli...  17.4 us
    all_to_all x1, blocking collectives, body(): lax.all_to_all(result.reshape(tp_size, experts * capacity, -1), 'tp', spl...  17.3 us
  transfers between devices with their start and end apart: 5, of which 4 were waited for; matrix products, arithmetic and copies ran while one was open for 1% of the time, Pallas kernels for 0%

profile of v1, /device:TPU:1, one launch (start us, length us, event | category | flops | bytes accessed | tf_op | source)
XLA Modules:
  0.0 477.9 jit_solution(17198584147014565074)
XLA Ops:
  6.5 0.7 slice.359
  7.4 3.9 collective-permute-start
  11.4 0.8 slice_bitcast_fusion.3
  12.2 0.7 fusion.50
  12.9 1.0 copy.87
  13.9 1.1 copy.89
  15.0 1.0 copy.85
  16.5 1.0 fusion.12
  17.5 1.0 fusion.15
  19.0 4.5 slice.371
  23.5 4.5 slice.372
  27.9 4.5 slice.370
  32.4 5.0 %slice.374 = f32[256,128]{0,1:T(8,128)S(1)} slice(f32[512,128]{0,1:T(8,128)S(1)} %get-tuple-element.10), slice={[0:511:2], [0:128:1]} | slice | bytes 262144 | tf_op jit(solution)/shard_map/slice | solution.py:166
  37.5 2.2 slice.377
  39.7 2.2 slice.378
  41.9 2.2 slice.376
  44.1 2.2 slice.380
  46.3 1.1 slice.383
  47.5 1.2 slice.384
  48.6 1.2 slice.382
  49.8 1.1 slice.386
  52.2 0.8 slice.388
  57.0 0.8 add_multiply_fusion.15
  60.3 1.1 slice.381
  61.5 1.1 slice.430
  62.6 2.2 slice.375
  64.8 2.2 slice.432
  67.1 4.5 slice.369
  71.5 4.9 %slice.434 = f32[255,128]{0,1:T(8,128)S(1)} slice(f32[512,128]{0,1:T(8,128)S(1)} %get-tuple-element.9), slice={[2:512:2], [0:128:1]} | slice | bytes 261120 | tf_op jit(solution)/shard_map/slice | solution.py:166
  76.5 0.9 copy.116
  84.9 1.1 pad.140
  86.0 1.1 pad.141
  87.2 1.1 pad.123
  88.4 1.1 pad.122
  89.7 2.2 pad.142
  91.9 2.2 pad.143
  94.1 4.5 pad.145
  98.7 2.2 pad.124
  100.9 2.2 pad.125
  103.3 4.4 pad.144
  107.9 4.6 pad.127
  112.6 4.4 pad.126
  117.1 0.6 broadcast_in_dim.64
  117.8 12.6 %all-to-all-start = ((f32[32,2,128]{2,1,0:T(2,128)}), f32[32,2,128]{2,1,0:T(2,128)S(1)}, u32[]{:S(2)}, u32[]{:S(2)}) async-start(f32[32,2,128]{2,1,0:T(2,128)} %broadcast_in_dim.64), calls=%async_computation | async-start | bytes 65536 | tf_op jit(solution)/shard_map/all_to_all | solution.py:18
  130.4 8.7 %all-to-all-done = f32[32,2,128]{2,1,0:T(2,128)S(1)} async-done(((f32[32,2,128]{2,1,0:T(2,128)}), f32[32,2,128]{2,1,0:T(2,128)S(1)}, u32[]{:S(2)}, u32[]{:S(2)}) %all-to-all-start) | async-done | bytes 32800 | tf_op jit(solution)/shard_map/all_to_all | solution.py:18
  139.5 2.2 convolution_convert_fusion
  141.7 9.5 %all-to-all-start.1 = ((bf16[16,32,2048]{2,1,0:T(8,128)(2,1)}), bf16[16,32,2048]{2,1,0:T(8,128)(2,1)S(1)}, u32[]{:S(2)}, u32[]{:S(2)}) async-start(bf16[16,32,2048]{2,1,0:T(8,128)(2,1)} %bitcast.12), calls=%async_computation.1 | async-start | bytes 4194304 | tf_op jit(solution)/shard_map/all_to_all | solution.py:67
  151.2 0.8 broadcast_multiply_fusion
  152.9 47.3 %all-to-all-done.1 = bf16[16,32,2048]{2,1,0:T(8,128)(2,1)S(1)} async-done(((bf16[16,32,2048]{2,1,0:T(8,128)(2,1)}), bf16[16,32,2048]{2,1,0:T(8,128)(2,1)S(1)}, u32[]{:S(2)}, u32[]{:S(2)}) %all-to-all-start.1) | async-done | bytes 2097184 | tf_op jit(solution)/shard_map/all_to_all | solution.py:67
  200.9 0.8 gather_fusion
  202.3 19.9 %all_to_all.40 = bf16[32,3,2048]{2,1,0:T(4,128)(2,1)S(1)} all-to-all(bf16[32,3,2048]{2,1,0:T(4,128)(2,1)S(1)} %broadcast_select_fusion), channel_id=1, replica_groups=mesh['sp'=32,'tp'=16] {'sp'}, dimensions={0} | all-to-all | bytes 786432 | tf_op jit(solution)/shard_map/all_to_all | solution.py:197
  222.1 1.1 all_gather_reshape.3
  223.2 44.0 %all-gather.2.cloned.1.call-done = bf16[16,1,96,2048]{3,2,1,0:T(8,128)(2,1)} async-done(((bf16[1,1,96,2048]{3,2,1,0:T(8,128)(2,1)}), bf16[16,1,96,2048]{3,2,1,0:T(8,128)(2,1)}) %all-gather.2.cloned.1.call-update) | async-done | bytes 6291472 | tf_op jit(solution)/shard_map/all_gather | solution.py:81
  267.2 4.7 fusion.2
  272.0 1.8 fusion.7
  274.6 145.3 %all_to_all.41 = bf16[16,1536,128]{1,2,0:T(8,128)(2,1)S(1)} all-to-all(bf16[16,1536,128]{1,2,0:T(8,128)(2,1)S(1)} %stack.3), channel_id=1, replica_groups=mesh['sp'=32,'tp'=16] {'tp'}, dimensions={0} | all-to-all | bytes 12582912 | tf_op jit(solution)/shard_map/all_to_all | solution.py:114
  420.0 1.8 convolution_convert_fusion.1
  421.8 17.3 %all_to_all.42 = bf16[16,96,128]{2,1,0:T(8,128)(2,1)S(1)} all-to-all(bf16[16,96,128]{2,1,0:T(8,128)(2,1)S(1)} %bitcast.101), channel_id=1, replica_groups=mesh['sp'=32,'tp'=16] {'tp'}, dimensions={0} | all-to-all | bytes 786432 | tf_op jit(solution)/shard_map/all_to_all | solution.py:209
  439.3 0.9 reshape.173
  440.2 9.9 %all-to-all-start.5 = ((bf16[32,3,2048]{2,1,0:T(4,128)(2,1)}), bf16[32,3,2048]{2,1,0:T(4,128)(2,1)S(1)}, u32[]{:S(2)}, u32[]{:S(2)}) async-start(bf16[32,3,2048]{2,1,0:T(4,128)(2,1)} %reshape.173), calls=%async_computation.5 | async-start | bytes 1048576 | tf_op jit(solution)/shard_map/all_to_all | solution.py:216
  450.4 17.4 %all-to-all-done.5 = bf16[32,3,2048]{2,1,0:T(4,128)(2,1)S(1)} async-done(((bf16[32,3,2048]{2,1,0:T(4,128)(2,1)}), bf16[32,3,2048]{2,1,0:T(4,128)(2,1)S(1)}, u32[]{:S(2)}, u32[]{:S(2)}) %all-to-all-start.5) | async-done | bytes 393248 | tf_op jit(solution)/shard_map/all_to_all | solution.py:216
  468.1 0.7 gather_fusion.1
  469.2 0.7 multiply_reduce_fusion
  469.9 0.7 fusion.22
  (191 shorter events, 21.3 us)
Async XLA Ops:
  6.5 133.0 %copy-start = (bf16[128,2048]{1,0:T(8,128)(2,1)S(1)}, bf16[128,2048]{1,0:T(8,128)(2,1)}, u32[]{:S(2)}) copy-start(bf16[128,2048]{1,0:T(8,128)(2,1)} %param.23) | copy-start | bytes 1572868
  7.4 8.6 %collective-permute-start = (bf16[3,128]{0,1:T(8,128)(2,1)S(1)}, bf16[3,128]{0,1:T(8,128)(2,1)S(1)}, u32[]{:S(2)}, u32[]{:S(2)}) collective-permute-start(bf16[3,128]{0,1:T(8,128)(2,1)S(1)} %copy.86), channel_id=1, source_target_pairs={{0,16},{16,32},{32,48},{48,64},{64,80},{80,96},{96,112},{112,128},... | collective-permute-start | bytes 2312 | tf_op jit(solution)/shard_map/ppermute | solution.py:13
  107.8 92.8 %copy-start.1 = (bf16[32,2048]{1,0:T(8,128)(2,1)S(1)}, bf16[32,2048]{1,0:T(8,128)(2,1)}, u32[]{:S(2)}) copy-start(bf16[32,2048]{1,0:T(8,128)(2,1)} %param.15) | copy-start | bytes 393220
  112.4 88.3 %copy-start.2 = (f32[2048]{0:T(1024)S(1)}, f32[2048]{0:T(1024)}, u32[]{:S(2)}) copy-start(f32[2048]{0:T(1024)} %param.24) | copy-start | bytes 24580
  117.8 21.3 %all-to-all-start = ((f32[32,2,128]{2,1,0:T(2,128)}), f32[32,2,128]{2,1,0:T(2,128)S(1)}, u32[]{:S(2)}, u32[]{:S(2)}) async-start(f32[32,2,128]{2,1,0:T(2,128)} %broadcast_in_dim.64), calls=%async_computation | async-start | bytes 65536 | tf_op jit(solution)/shard_map/all_to_all | solution.py:18
  141.7 58.5 %all-to-all-start.1 = ((bf16[16,32,2048]{2,1,0:T(8,128)(2,1)}), bf16[16,32,2048]{2,1,0:T(8,128)(2,1)S(1)}, u32[]{:S(2)}, u32[]{:S(2)}) async-start(bf16[16,32,2048]{2,1,0:T(8,128)(2,1)} %bitcast.12), calls=%async_computation.1 | async-start | bytes 4194304 | tf_op jit(solution)/shard_map/all_to_all | solution.py:67
  151.2 116.1 %copy-start.5 = (bf16[1,2048,128]{2,1,0:T(8,128)(2,1)S(1)}, bf16[1,2048,128]{2,1,0:T(8,128)(2,1)}, u32[]{:S(2)}) copy-start(bf16[1,2048,128]{2,1,0:T(8,128)(2,1)} %param.27) | copy-start | bytes 1572868
  151.2 116.0 %all-gather.2.cloned.1.call-start = ((), (), s32[]{:S(2)}) async-start(), calls=%async_computation.6 | async-start | bytes 6684672 | tf_op jit(solution)/shard_map/all_gather | solution.py:81
  223.2 48.8 %copy-start.6 = (bf16[1,2048,128]{2,1,0:T(8,128)(2,1)S(1)}, bf16[1,2048,128]{2,1,0:T(8,128)(2,1)}, u32[]{:S(2)}) copy-start(bf16[1,2048,128]{2,1,0:T(8,128)(2,1)} %param.28) | copy-start | bytes 1572868
  267.2 4.8 copy-start.4
  274.6 145.4 %copy-start.7 = (bf16[1,2048,128]{2,1,0:T(8,128)(2,1)S(1)}, bf16[1,2048,128]{2,1,0:T(8,128)(2,1)}, u32[]{:S(2)}) copy-start(bf16[1,2048,128]{2,1,0:T(8,128)(2,1)} %param.29) | copy-start | bytes 1572868
  420.0 30.3 %copy-start.3 = (f32[32,2]{0,1:T(2,128)S(1)}, f32[32,2]{0,1:T(2,128)}, u32[]{:S(2)}) copy-start(f32[32,2]{0,1:T(2,128)} %param.26) | copy-start | bytes 772
  440.2 27.6 %all-to-all-start.5 = ((bf16[32,3,2048]{2,1,0:T(4,128)(2,1)}), bf16[32,3,2048]{2,1,0:T(4,128)(2,1)S(1)}, u32[]{:S(2)}, u32[]{:S(2)}) async-start(bf16[32,3,2048]{2,1,0:T(4,128)(2,1)} %reshape.173), calls=%async_computation.5 | async-start | bytes 1048576 | tf_op jit(solution)/shard_map/all_to_all | solution.py:216
Sparse Core Ops, SparseCore 0:
  223.4 43.8 all-gather.1
